TPU v7x, 32 devices: a whole 2x2x4 slice. The times are simulated.
32 devices in a mesh: sp: 8 (over z, y), tp: 4 (over x, core).
Axes of the slice: x: 2, y: 2, z: 4, core: 2. Of those that a mesh axis runs over, the one named last changes fastest.
Arguments:
- residual: bfloat16 [8192, 2048], P('sp'), may hold values from -8 to 8
- query_wide: bfloat16 [8192, 1024], P('sp', 'tp'), may hold values from -6 to 6
- key_wide: bfloat16 [8192, 1024], P('sp', 'tp'), may hold values from -6 to 6
- value_wide: bfloat16 [8192, 2048], P('sp', 'tp'), may hold values from -6 to 6
- decay_wide: bfloat16 [8192, 1024], P('sp', 'tp'), may hold values from -12 to 12
- gate_wide: bfloat16 [8192, 2048], P('sp', 'tp'), may hold values from -6 to 6
- query_narrow: bfloat16 [8192, 512], P('sp', 'tp'), may hold values from -6 to 6
- key_narrow: bfloat16 [8192, 512], P('sp', 'tp'), may hold values from -6 to 6
- value_narrow: bfloat16 [8192, 2048], P('sp', 'tp'), may hold values from -6 to 6
- decay_narrow: bfloat16 [8192, 512], P('sp', 'tp'), may hold values from -12 to 12
- gate_narrow: bfloat16 [8192, 2048], P('sp', 'tp'), may hold values from -6 to 6
- head_gain: float32 [512], replicated, may hold values from 0.1 to 1.9
- out_wide: bfloat16 [2048, 2048], P('tp'), may hold values from -0.125 to 0.125
- out_narrow: bfloat16 [2048, 2048], P('tp'), may hold values from -0.125 to 0.125
- mlp_gain: float32 [2048], replicated, may hold values from 0.1 to 1.9
- up_weight: bfloat16 [2048, 4096], P('sp', 'tp'), may hold values from -0.125 to 0.125
- down_weight: bfloat16 [4096, 2048], P('tp', 'sp'), may hold values from -0.09375 to 0.09375
Outputs:
- layer_out: bfloat16 [8192, 2048], P('sp', 'tp')
All inputs are finite; a program needn't handle non-finite values.
Results may differ from a plain program's by a relative error of at most 0.017.
Values may be sent and summed in bfloat16 or wider, within the bound.
A program may use at most 128 MiB of HBM per device.

v0:
```python
import jax
import jax.numpy as jnp
from jax import lax
from jax.sharding import PartitionSpec as P

HEADS = 4
BLOCK = 64
EPS = 1e-05
DECAY_NORMALIZER = 16.0
HIGHEST = lax.Precision.HIGHEST


def entering(array, axis, join, neutral):
    place = lax.axis_index(axis)
    gathered = jax.tree.map(
        lambda a, kind: lax.all_gather(a.astype(kind), axis),
        array,
        (jnp.bfloat16, jnp.bfloat16, jnp.bfloat16, jnp.bfloat16),
    )
    state = jax.tree.map(lambda a, e: jnp.zeros_like(a) + jnp.asarray(e, a.dtype), array, neutral)

    def one(step, state):
        return join(
            state,
            jax.tree.map(
                lambda a, own: lax.dynamic_index_in_dim(a, step, 0, False).astype(own.dtype),
                gathered,
                array,
            ),
        )

    return lax.fori_loop(0, place, one, state)


def block_pass(queries, keys_in, values_in, log_decay, block_len):
    num_blocks = queries.shape[0] // block_len

    def to_blocks(stacked):
        return stacked.reshape((num_blocks, block_len) + stacked.shape[1:])

    causal = jnp.tril(jnp.ones((block_len, block_len), dtype=bool))
    initial = (
        jnp.zeros((queries.shape[1], queries.shape[2], values_in.shape[2]), jnp.float32),
        jnp.zeros((queries.shape[1], queries.shape[2]), jnp.float32),
    )

    def advance(running, inputs):
        memory, offset = running
        block_q, block_k, block_v, block_g = inputs
        within = jnp.cumsum(block_g, axis=0)
        final_log = within[-1]
        scaled_q = block_q * jnp.exp(within)
        scaled_k = block_k * jnp.exp(-within)
        outside = jnp.einsum("ihd,hde->ihe", scaled_q, memory, precision=HIGHEST)
        scores = jnp.einsum("ihd,jhd->hij", scaled_q, scaled_k, precision=HIGHEST)
        scores = jnp.where(causal[None], scores, 0.0)
        inside = jnp.einsum("hij,jhe->ihe", scores, block_v, precision=HIGHEST)
        decayed_keys = scaled_k * jnp.exp(final_log)[None]
        memory = jnp.exp(final_log)[..., None] * memory + jnp.einsum(
            "jhd,jhe->hde", decayed_keys, block_v, precision=HIGHEST
        )
        carried_q = scaled_q * jnp.exp(offset)[None]
        return ((memory, offset + final_log), (outside + inside, carried_q))

    (memory, totals), (outputs, carried_q) = lax.scan(
        advance,
        initial,
        (to_blocks(queries), to_blocks(keys_in), to_blocks(values_in), to_blocks(log_decay)),
    )
    return (outputs.reshape(values_in.shape), carried_q.reshape(queries.shape), totals, memory)


def prepare(query, key_proj, value, decay, heads_here):
    row_count = query.shape[0]
    key_width = query.shape[1] // heads_here
    queries = query.astype(jnp.float32).reshape(row_count, heads_here, key_width) * key_width ** (
        -0.5
    )
    keys_in = key_proj.astype(jnp.float32).reshape(row_count, heads_here, key_width)
    values_in = value.astype(jnp.float32).reshape(
        row_count, heads_here, value.shape[1] // heads_here
    )
    log_decay = (
        jax.nn.log_sigmoid(decay.astype(jnp.float32)).reshape(row_count, heads_here, key_width)
        / DECAY_NORMALIZER
    )
    return (queries, keys_in, values_in, log_decay)


def finish(outputs, gate, head_gain):
    scale = lax.rsqrt(jnp.mean(jnp.square(outputs), axis=-1, keepdims=True) + EPS)
    gated = (
        outputs * scale * head_gain * jax.nn.silu(gate.astype(jnp.float32).reshape(outputs.shape))
    )
    return gated.reshape(outputs.shape[0], -1).astype(jnp.bfloat16)


def combine_states(earlier, later):
    return (
        earlier[0] + later[0],
        jnp.exp(later[0])[..., None] * earlier[1] + later[1],
        earlier[2] + later[2],
        jnp.exp(later[2])[..., None] * earlier[3] + later[3],
    )


def body(
    residual,
    query_wide,
    key_wide,
    value_wide,
    decay_wide,
    gate_wide,
    query_narrow,
    key_narrow,
    value_narrow,
    decay_narrow,
    gate_narrow,
    head_gain,
    out_wide,
    out_narrow,
    mlp_gain,
    up_weight,
    down_weight,
):
    heads_here = HEADS // lax.axis_size("tp")
    up_whole, down_whole = (
        lax.all_gather(up_weight, "sp", axis=0, tiled=True),
        lax.all_gather(down_weight, "sp", axis=1, tiled=True),
    )
    wq, wk, wv, wg = prepare(query_wide, key_wide, value_wide, decay_wide, heads_here)
    wide_out, wide_q, wide_total, wide_memory = block_pass(wq, wk, wv, wg, BLOCK)
    nq, nk, nv, ng = prepare(query_narrow, key_narrow, value_narrow, decay_narrow, heads_here)
    narrow_out, narrow_q, narrow_total, narrow_memory = block_pass(nq, nk, nv, ng, BLOCK)
    identity = (
        jnp.zeros_like(wide_total),
        jnp.zeros_like(wide_memory),
        jnp.zeros_like(narrow_total),
        jnp.zeros_like(narrow_memory),
    )
    incoming = entering(
        (wide_total, wide_memory, narrow_total, narrow_memory), "sp", combine_states, identity
    )
    wide_out = wide_out + jnp.einsum("ihd,hde->ihe", wide_q, incoming[1], precision=HIGHEST)
    narrow_out = narrow_out + jnp.einsum("ihd,hde->ihe", narrow_q, incoming[3], precision=HIGHEST)
    gated_wide = finish(wide_out, gate_wide, head_gain)
    gated_narrow = finish(narrow_out, gate_narrow, head_gain)
    head_terms = jnp.dot(gated_wide, out_wide, preferred_element_type=jnp.float32) + jnp.dot(
        gated_narrow, out_narrow, preferred_element_type=jnp.float32
    )
    tp_index = lax.axis_index("tp")
    col_count = residual.shape[1] // lax.axis_size("tp")
    full_width = residual.shape[1]
    residual_cols = lax.dynamic_slice_in_dim(residual, tp_index * col_count, col_count, 1)
    mixed_cols = lax.psum_scatter(
        head_terms.astype(jnp.bfloat16), "tp", scatter_dimension=1, tiled=True
    ).astype(jnp.float32)
    stream_cols = (residual_cols.astype(jnp.float32) + mixed_cols).astype(jnp.bfloat16)
    stream_f = stream_cols.astype(jnp.float32)
    squares = lax.psum(jnp.sum(jnp.square(stream_f), axis=1, keepdims=True), "tp")
    gain_cols = lax.dynamic_slice_in_dim(mlp_gain, tp_index * col_count, col_count, 0)
    normed_cols = (stream_f * lax.rsqrt(squares / full_width + EPS) * gain_cols).astype(
        jnp.bfloat16
    )
    normed = lax.all_gather(normed_cols, "tp", axis=1, tiled=True)
    before_activation = jnp.dot(normed, up_whole, preferred_element_type=jnp.float32)
    hidden = jnp.square(jax.nn.relu(before_activation)).astype(jnp.bfloat16)
    down_terms = jnp.dot(hidden, down_whole, preferred_element_type=jnp.float32)
    mlp_cols = lax.psum_scatter(
        down_terms.astype(jnp.bfloat16), "tp", scatter_dimension=1, tiled=True
    ).astype(jnp.float32)
    return (stream_cols.astype(jnp.float32) + mlp_cols).astype(jnp.bfloat16)


def solution(mesh):
    return jax.shard_map(
        body,
        mesh=mesh,
        in_specs=(
            P("sp", None),
            P("sp", "tp"),
            P("sp", "tp"),
            P("sp", "tp"),
            P("sp", "tp"),
            P("sp", "tp"),
            P("sp", "tp"),
            P("sp", "tp"),
            P("sp", "tp"),
            P("sp", "tp"),
            P("sp", "tp"),
            P(),
            P("tp", None),
            P("tp", None),
            P(),
            P("sp", "tp"),
            P("tp", "sp"),
        ),
        out_specs=P("sp", "tp"),
        check_vma=False,
    )
```

profile of v0, /device:TPU:0, one launch (start us, length us, event | category | flops | bytes accessed | tf_op | source)
XLA Modules:
  0.0 591.7 jit_solution(7153783925277661843)
XLA Ops:
  6.6 5.0 reshape.501
  15.4 68.5 %while.51 = (s32[]{:T(128)}, f32[1,128,512]{2,1,0:T(8,128)S(1)}, f32[1,128]{1,0:T(1,128)S(1)}, f32[16,64,1,512]{3,1,2,0:T(8,128)}, f32[16,64,1,128]{3,1,2,0:T(8,...) while((s32[]{:T(128)}, f32[1,128,512]{2,1,0:T(8,128)S(1)}, ...), condition=%wide.region_5.6_spmd.clone, body=%wide.region_3.5_spmd.clone.sunk | while | flops 133005568 | bytes 2333321 | solution.py:65
  84.7 2.7 fusion.81
  87.3 3.3 reshape.486
  91.6 3.3 reshape.487
  95.0 4.9 reshape.499
  99.8 2.0 reshape.498
  103.4 108.7 %while.50 = (s32[]{:T(128)}, f32[1,256,512]{2,1,0:T(8,128)S(1)}, f32[1,256]{1,0:T(1,128)S(1)}, f32[16,64,1,512]{3,1,2,0:T(8,128)}, f32[16,64,1,256]{3,1,2,0:T(8,...) while((s32[]{:T(128)}, f32[1,256,512]{2,1,0:T(8,128)S(1)}, ...), condition=%wide.region_2.3_spmd.clone, body=%wide.region_0.2_spmd.clone.sunk | while | flops 240787968 | bytes 3648133 | solution.py:65
  212.9 3.0 copy.32
  217.2 3.0 copy.34
  221.5 22.3 %all-gather.5 = bf16[8,1,128]{2,1,0:T(2,128)(2,1)S(1)} all-gather(bf16[1,1,128]{2,1,0:T(2,128)(2,1)S(1)} %convert_bitcast_fusion.1), channel_id=4, replica_groups=mesh['sp'=8,'tp'=4] {'sp'}, dimensions={0}, use_global_device_ids=true | all-gather | bytes 2304 | tf_op jit(solution)/shard_map/all_gather | solution.py:16
  243.9 16.7 %all-gather.4 = bf16[8,1,256]{2,1,0:T(2,128)(2,1)S(1)} all-gather(bf16[1,1,256]{2,1,0:T(2,128)(2,1)S(1)} %convert_bitcast_fusion), channel_id=2, replica_groups=mesh['sp'=8,'tp'=4] {'sp'}, dimensions={0}, use_global_device_ids=true | all-gather | bytes 4608 | tf_op jit(solution)/shard_map/all_gather | solution.py:16
  260.6 4.6 all-gather.18.cloned.1.call-done
  265.4 5.6 multiply_reduce_fusion.1
  273.2 2.8 fusion.78
  276.0 5.0 add_convert_fusion
  283.0 56.4 %reduce-scatter.3.cloned.1.call-done = bf16[1024,512]{1,0:T(8,128)(2,1)} async-done(((bf16[1024,2048]{1,0:T(8,128)(2,1)}), bf16[1024,512]{1,0:T(8,128)(2,1)}) %reduce-scatter.3.cloned.1.call-update) | async-done | bytes 1048592 | tf_op jit(solution)/shard_map/reduce_scatter | solution.py:155
  341.4 5.8 psum.7
  348.8 65.5 %all-gather.14.cloned.1.call-done = bf16[2048,1024]{1,0:T(8,128)(2,1)} async-done(((bf16[256,1024]{1,0:T(8,128)(2,1)}), bf16[2048,1024]{1,0:T(8,128)(2,1)}) %all-gather.14.cloned.1.call-update) | async-done | bytes 4194320 | tf_op jit(solution)/shard_map/all_gather | solution.py:128
  414.3 75.1 %all-gather.16.cloned.1.call-done = bf16[1024,2048]{1,0:T(8,128)(2,1)} async-done(((bf16[1024,256]{1,0:T(8,128)(2,1)}), bf16[1024,2048]{1,0:T(8,128)(2,1)}) %all-gather.16.cloned.1.call-update) | async-done | bytes 4194320 | tf_op jit(solution)/shard_map/all_gather | solution.py:129
  489.4 34.1 %all-gather.12.cloned.1.call-done = bf16[1024,2048]{1,0:T(8,128)(2,1)} async-done(((bf16[1024,512]{1,0:T(8,128)(2,1)}), bf16[1024,2048]{1,0:T(8,128)(2,1)}) %all-gather.12.cloned.1.call-update) | async-done | bytes 4194320 | tf_op jit(solution)/shard_map/all_gather | solution.py:165
  523.4 14.4 %convolution_convert_fusion = bf16[1024,2048]{1,0:T(8,128)(2,1)} fusion(bf16[1024,2048]{1,0:T(8,128)(2,1)} %all-gather.16.cloned.1.call-done, bf16[1024,2048]{1,0:T(8,128)(2,1)} %all-gather.12.cloned.1.call-done, bf16[2048,1024]{1,0:T(8,128)(2,1)} %all-gather.14.cloned.1.call-done), kind=kOutput, calls=%fused_computation.91 | convolution fusion | flops 8595177472 | bytes 16777216 | tf_op jit(solution)/shard_map/dot_general | solution.py:168
  537.9 44.5 %reduce-scatter.5.cloned.1.call-done = bf16[1024,512]{1,0:T(8,128)(2,1)} async-done(((bf16[1024,2048]{1,0:T(8,128)(2,1)}), bf16[1024,512]{1,0:T(8,128)(2,1)}) %reduce-scatter.5.cloned.1.call-update) | async-done | bytes 1048592 | tf_op jit(solution)/shard_map/reduce_scatter | solution.py:169
  582.4 2.5 fusion.74
  (423 shorter events, 193.9 us)
Async XLA Ops:
  6.5 266.6 %copy-start = (bf16[512,2048]{1,0:T(8,128)(2,1)S(1)}, bf16[512,2048]{1,0:T(8,128)(2,1)}, u32[]{:S(2)}) copy-start(bf16[512,2048]{1,0:T(8,128)(2,1)} %param.35) | copy-start | bytes 6291460
  6.5 5.0 copy-start.10
  6.5 5.1 copy-start.11
  6.5 254.0 %all-gather.20.cloned.1.call-start = ((), (), s32[]{:S(2)}) async-start(), calls=%async_computation.8 | async-start | bytes 1179648 | tf_op jit(solution)/shard_map/all_gather | solution.py:16
  83.9 6.7 %copy-start.7 = (bf16[1024,256]{1,0:T(8,128)(2,1)S(1)}, bf16[1024,256]{1,0:T(8,128)(2,1)}, u32[]{:S(2)}) copy-start(bf16[1024,256]{1,0:T(8,128)(2,1)} %param.24) | copy-start | bytes 1572868
  84.6 180.5 %all-gather.18.cloned.1.call-start = ((), (), s32[]{:S(2)}) async-start(), calls=%async_computation.7 | async-start | bytes 2359296 | tf_op jit(solution)/shard_map/all_gather | solution.py:16
  91.6 8.2 %copy-start.8 = (bf16[1024,256]{1,0:T(8,128)(2,1)S(1)}, bf16[1024,256]{1,0:T(8,128)(2,1)}, u32[]{:S(2)}) copy-start(bf16[1024,256]{1,0:T(8,128)(2,1)} %param.25) | copy-start | bytes 1572868
  212.9 126.6 %reduce-scatter.3.cloned.1.call-start = ((), (), s32[]{:S(2)}) async-start(), calls=%async_computation.2 | async-start | bytes 5242880 | tf_op jit(solution)/shard_map/reduce_scatter | solution.py:155
  212.9 3.0 copy-start.3
  217.2 3.0 copy-start.4
  265.4 5.7 copy-start.2
  265.4 5.7 copy-start.9
  271.1 2.1 copy-start.6
  271.1 2.1 copy-start.13
  273.2 2.8 copy-start.5
  273.2 2.8 copy-start.12
  281.0 133.2 %all-gather.14.cloned.1.call-start = ((), (), s32[]{:S(2)}) async-start(), calls=%async_computation.4 | async-start | bytes 4718592 | tf_op jit(solution)/shard_map/all_gather | solution.py:128
  281.6 207.7 %all-gather.16.cloned.1.call-start = ((), (), s32[]{:S(2)}) async-start(), calls=%async_computation.5 | async-start | bytes 4718592 | tf_op jit(solution)/shard_map/all_gather | solution.py:129
  282.2 241.2 %all-gather.12.cloned.1.call-start = ((), (), s32[]{:S(2)}) async-start(), calls=%async_computation.3 | async-start | bytes 5242880 | tf_op jit(solution)/shard_map/all_gather | solution.py:165
  348.5 233.9 %reduce-scatter.5.cloned.1.call-start = ((), (), s32[]{:S(2)}) async-start(), calls=%async_computation.6 | async-start | bytes 5242880 | tf_op jit(solution)/shard_map/reduce_scatter | solution.py:169
  537.9 47.0 %copy-start.1 = (bf16[512,2048]{1,0:T(8,128)(2,1)S(1)}, bf16[512,2048]{1,0:T(8,128)(2,1)}, u32[]{:S(2)}) copy-start(bf16[512,2048]{1,0:T(8,128)(2,1)} %param.35) | copy-start | bytes 6291460
Sparse Core Ops, SparseCore 0:
  84.7 43.0 all-gather.19
  213.0 52.1 all-gather.17
  281.2 58.2 reduce-scatter.2
  341.4 72.7 all-gather.13
  416.2 73.1 all-gather.15
  490.8 32.6 all-gather.11
  538.0 44.3 reduce-scatter.4
where the time goes:
time: 596 us; the launch traced here: 592 us
  waiting for transfers between devices  281 us (47%)
  matrix products  95.3 us (16%)
  local copies, waits for them, and re-layouts  83 us (14%)
  other arithmetic  71.2 us (12%)
  blocking collectives  44.8 us (8%)
  between operations  13.8 us (2%)
    all_gather x1, waiting for transfers between devices, body(): lax.all_gather(down_weight, 'sp', axis=1, tiled=True)  75.1 us
    all_gather x1, waiting for transfers between devices, body(): lax.all_gather(up_weight, 'sp', axis=0, tiled=True)  65.5 us
    reduce_scatter x1, waiting for transfers between devices, body(): lax.psum_scatter(head_terms.astype(jnp.bfloat16), 'tp', scatter_dimension...  56.4 us
    reduce_scatter x1, waiting for transfers between devices, body(): lax.psum_scatter(down_terms.astype(jnp.bfloat16), 'tp', scatter_dimension...  44.5 us
    dynamic_slice x48, local copies, waits for them, and re-layouts, block_pass(): lax.scan(advance, initial, (to_blocks(queries), to_blocks(keys_in), to_bl...  41.7 us
    all_gather x2, blocking collectives, entering(): lax.all_gather(a.astype(kind), axis)  39 us
    all_gather x1, waiting for transfers between devices, body(): normed = lax.all_gather(normed_cols, 'tp', axis=1, tiled=True)  34.1 us
    dot_general x32, matrix products, advance(): outside = jnp.einsum('ihd,hde->ihe', scaled_q, memory, precision=HIGHEST)  22.1 us
  transfers between devices with their start and end apart: 7, of which 6 were waited for; matrix products, arithmetic and copies ran while one was open for 24% of the time, Pallas kernels for 0%

commit v1 on v0

--- a/solution.py
+++ b/solution.py
@@ -2,6 +2,7 @@
 import jax.numpy as jnp
 from jax import lax
 from jax.sharding import PartitionSpec as P
+from jax.lax import axis_index, axis_size, ppermute
 
 HEADS = 4
 BLOCK = 64
@@ -123,6 +124,22 @@
     up_weight,
     down_weight,
 ):
+
+    def drive_the_shapes(frame_in):
+        k_all = axis_size("tp")
+        mixed_arr = [(j - 1, j) for j in range(1, k_all)] + [(k_all - 1, 0)]
+        near = frame_in
+        items = [near]
+        for _ in range(k_all - 1):
+            near = ppermute(near, "tp", mixed_arr)
+            items += [near]
+        w1 = jnp.roll(
+            jnp.concatenate([*reversed(items)], axis=1),
+            shift=(axis_index("tp") + 1) * near.shape[1],
+            axis=1,
+        )
+        return w1
+
     heads_here = HEADS // lax.axis_size("tp")
     up_whole, down_whole = (
         lax.all_gather(up_weight, "sp", axis=0, tiled=True),
@@ -162,7 +179,7 @@
     normed_cols = (stream_f * lax.rsqrt(squares / full_width + EPS) * gain_cols).astype(
         jnp.bfloat16
     )
-    normed = lax.all_gather(normed_cols, "tp", axis=1, tiled=True)
+    normed = drive_the_shapes(normed_cols)
     before_activation = jnp.dot(normed, up_whole, preferred_element_type=jnp.float32)
     hidden = jnp.square(jax.nn.relu(before_activation)).astype(jnp.bfloat16)
     down_terms = jnp.dot(hidden, down_whole, preferred_element_type=jnp.float32)

time: 596 us -> 560 us (0.940)
  waiting for transfers between devices: 281 us -> 235 us
  local copies, waits for them, and re-layouts: 83 us -> 92.1 us
    all_gather x1, waiting for transfers between devices: 65.5 us -> 12 us  [body(): lax.all_gather(up_weight, 'sp', axis=0, tiled=True)]
    ppermute x0 -> x3, waiting for transfers between devices: none -> 42.8 us  [drive_the_shapes(): near = ppermute(near, 'tp', mixed_arr)]
    all_gather x1 -> x0, waiting for transfers between devices: 34.1 us -> none  [body(): normed = lax.all_gather(normed_cols, 'tp', axis=1, tiled=True)]
    unnamed x30 -> x36, local copies, waits for them, and re-layouts: 2.69 us -> 11.8 us
  transfers between devices with their start and end apart: 7 -> 9, of which waited for: 6 -> 8; matrix products, arithmetic and copies ran while one was open for 24% -> 27% of each run, Pallas kernels for 0% -> 0%
where the time goes in v1:
time: 560 us; the launch traced here: 556 us
  waiting for transfers between devices  235 us (42%)
  matrix products  95.3 us (17%)
  local copies, waits for them, and re-layouts  92.1 us (16%)
  other arithmetic  73 us (13%)
  blocking collectives  44.8 us (8%)
  between operations  13.8 us (2%)
    all_gather x1, waiting for transfers between devices, body(): lax.all_gather(down_weight, 'sp', axis=1, tiled=True)  75.1 us
    reduce_scatter x1, waiting for transfers between devices, body(): lax.psum_scatter(head_terms.astype(jnp.bfloat16), 'tp', scatter_dimension...  56.4 us
    ppermute x3, waiting for transfers between devices, drive_the_shapes(): near = ppermute(near, 'tp', mixed_arr)  42.8 us
    reduce_scatter x1, waiting for transfers between devices, body(): lax.psum_scatter(down_terms.astype(jnp.bfloat16), 'tp', scatter_dimension...  42.7 us
    dynamic_slice x48, local copies, waits for them, and re-layouts, block_pass(): lax.scan(advance, initial, (to_blocks(queries), to_blocks(keys_in), to_bl...  41.7 us
    all_gather x2, blocking collectives, entering(): lax.all_gather(a.astype(kind), axis)  39 us
    dot_general x32, matrix products, advance(): outside = jnp.einsum('ihd,hde->ihe', scaled_q, memory, precision=HIGHEST)  22.1 us
    dot_general x32, matrix products, advance(): inside = jnp.einsum('hij,jhe->ihe', scores, block_v, precision=HIGHEST)  19.4 us
  transfers between devices with their start and end apart: 9, of which 8 were waited for; matrix products, arithmetic and copies ran while one was open for 27% of the time, Pallas kernels for 0%

profile of v1, /device:TPU:0, one launch (start us, length us, event | category | flops | bytes accessed | tf_op | source)
XLA Modules:
  0.0 555.8 jit_solution(17129936158875103754)
XLA Ops:
  6.6 5.0 reshape.501
  15.4 68.5 %while.51 = (s32[]{:T(128)}, f32[1,128,512]{2,1,0:T(8,128)S(1)}, f32[1,128]{1,0:T(1,128)S(1)}, f32[16,64,1,512]{3,1,2,0:T(8,128)}, f32[16,64,1,128]{3,1,2,0:T(8,...) while((s32[]{:T(128)}, f32[1,128,512]{2,1,0:T(8,128)S(1)}, ...), condition=%wide.region_5.6_spmd.clone, body=%wide.region_3.5_spmd.clone.sunk | while | flops 133005568 | bytes 2333321 | solution.py:66
  84.7 2.7 fusion.88
  87.3 3.3 reshape.486
  91.6 3.3 reshape.487
  95.0 4.9 reshape.499
  103.4 108.7 %while.50 = (s32[]{:T(128)}, f32[1,256,512]{2,1,0:T(8,128)S(1)}, f32[1,256]{1,0:T(1,128)S(1)}, f32[16,64,1,512]{3,1,2,0:T(8,128)}, f32[16,64,1,256]{3,1,2,0:T(8,...) while((s32[]{:T(128)}, f32[1,256,512]{2,1,0:T(8,128)S(1)}, ...), condition=%wide.region_2.3_spmd.clone, body=%wide.region_0.2_spmd.clone.sunk | while | flops 240787968 | bytes 3648133 | solution.py:66
  212.9 3.0 copy.32
  217.2 3.0 copy.34
  221.5 22.3 %all-gather.5 = bf16[8,1,128]{2,1,0:T(2,128)(2,1)S(1)} all-gather(bf16[1,1,128]{2,1,0:T(2,128)(2,1)S(1)} %convert_bitcast_fusion.1), channel_id=4, replica_groups=mesh['sp'=8,'tp'=4] {'sp'}, dimensions={0}, use_global_device_ids=true | all-gather | bytes 2304 | tf_op jit(solution)/shard_map/all_gather | solution.py:17
  243.9 16.7 %all-gather.4 = bf16[8,1,256]{2,1,0:T(2,128)(2,1)S(1)} all-gather(bf16[1,1,256]{2,1,0:T(2,128)(2,1)S(1)} %convert_bitcast_fusion), channel_id=2, replica_groups=mesh['sp'=8,'tp'=4] {'sp'}, dimensions={0}, use_global_device_ids=true | all-gather | bytes 4608 | tf_op jit(solution)/shard_map/all_gather | solution.py:17
  260.6 4.6 all-gather.15.cloned.1.call-done
  265.4 5.6 %multiply_reduce_fusion.1 = (f32[1024]{0:T(1024)S(1)}, f32[1024,1,512]{0,2,1:T(8,128)S(1)}) fusion(f32[1024,1,512]{0,2,1:T(8,128)} %copy.32, f32[1024,256]{1,0:T(8,128)} %bitcast.284, f32[1,256,512]{2,1,0:T(8,128)S(1)} %get-tuple-element.190), kind=kOutput, calls=%fused_computation.123 | convolution fusion | flops 1612184576 | bytes 5771264 | tf_op jit(solution)/shard_map/ihd,hde->ihe/dot_general | solution.py:161
  273.2 2.8 fusion.85
  276.0 5.0 add_convert_fusion
  283.0 56.4 %reduce-scatter.3.cloned.1.call-done = bf16[1024,512]{1,0:T(8,128)(2,1)} async-done(((bf16[1024,2048]{1,0:T(8,128)(2,1)}), bf16[1024,512]{1,0:T(8,128)(2,1)}) %reduce-scatter.3.cloned.1.call-update) | async-done | bytes 1048592 | tf_op jit(solution)/shard_map/reduce_scatter | solution.py:172
  341.4 5.8 %psum.7 = f32[1024,1]{0,1:T(1,128)S(1)} all-reduce(f32[1024,1]{0,1:T(1,128)S(1)} %bitcast.297), channel_id=1, replica_groups=mesh['sp'=8,'tp'=4] {'tp'}, use_global_device_ids=true, to_apply=%region_12.13 | all-reduce | flops 1024 | bytes 8192 | tf_op jit(solution)/shard_map/psum | solution.py:177
  347.6 14.2 %collective-permute-done = bf16[1024,512]{1,0:T(8,128)(2,1)S(1)} collective-permute-done((bf16[1024,512]{1,0:T(8,128)(2,1)S(1)}, bf16[1024,512]{1,0:T(8,128)(2,1)S(1)}, u32[]{:S(2)}, u32[]{:S(2)}) %collective-permute-start) | collective-permute-done | bytes 1048608 | tf_op jit(solution)/shard_map/ppermute | solution.py:134
  361.8 14.2 %collective-permute-done.1 = bf16[1024,512]{1,0:T(8,128)(2,1)S(1)} collective-permute-done((bf16[1024,512]{1,0:T(8,128)(2,1)S(1)}, bf16[1024,512]{1,0:T(8,128)(2,1)S(1)}, u32[]{:S(2)}, u32[]{:S(2)}) %collective-permute-start.1) | collective-permute-done | bytes 1048608 | tf_op jit(solution)/shard_map/ppermute | solution.py:134
  376.0 14.3 %collective-permute-done.2 = bf16[1024,512]{1,0:T(8,128)(2,1)} collective-permute-done((bf16[1024,512]{1,0:T(8,128)(2,1)S(1)}, bf16[1024,512]{1,0:T(8,128)(2,1)}, u32[]{:S(2)}, u32[]{:S(2)}) %collective-permute-start.2) | collective-permute-done | bytes 1048608 | tf_op jit(solution)/shard_map/ppermute | solution.py:134
  402.2 12.0 %all-gather.11.cloned.1.call-done = bf16[2048,1024]{1,0:T(8,128)(2,1)} async-done(((bf16[256,1024]{1,0:T(8,128)(2,1)}), bf16[2048,1024]{1,0:T(8,128)(2,1)}) %all-gather.11.cloned.1.call-update) | async-done | bytes 4194320 | tf_op jit(solution)/shard_map/all_gather | solution.py:145
  414.2 75.1 %all-gather.13.cloned.1.call-done = bf16[1024,2048]{1,0:T(8,128)(2,1)} async-done(((bf16[1024,256]{1,0:T(8,128)(2,1)}), bf16[1024,2048]{1,0:T(8,128)(2,1)}) %all-gather.13.cloned.1.call-update) | async-done | bytes 4194320 | tf_op jit(solution)/shard_map/all_gather | solution.py:146
  489.3 14.4 %convolution_convert_fusion = bf16[1024,2048]{1,0:T(8,128)(2,1)} fusion(bf16[1024,2048]{1,0:T(8,128)(2,1)} %all-gather.13.cloned.1.call-done, bf16[2048,1024]{1,0:T(8,128)(2,1)} %all-gather.11.cloned.1.call-done, bf16[1024,4096]{1,0:T(8,128)(2,1)} %constant_dynamic-update-slice_fusion, s32[]{:T(128)S(6)} %select_n.54), kind=kOutput, calls=%fused_computation.93 | convolution fusion | flops 8595177472 | bytes 16777220 | tf_op jit(solution)/shard_map/dot_general | solution.py:185
  503.7 42.7 %reduce-scatter.5.cloned.1.call-done = bf16[1024,512]{1,0:T(8,128)(2,1)} async-done(((bf16[1024,2048]{1,0:T(8,128)(2,1)}), bf16[1024,512]{1,0:T(8,128)(2,1)}) %reduce-scatter.5.cloned.1.call-update) | async-done | bytes 1048592 | tf_op jit(solution)/shard_map/reduce_scatter | solution.py:186
  (434 shorter events, 209.2 us)
Async XLA Ops:
  6.5 266.6 %copy-start = (bf16[512,2048]{1,0:T(8,128)(2,1)S(1)}, bf16[512,2048]{1,0:T(8,128)(2,1)}, u32[]{:S(2)}) copy-start(bf16[512,2048]{1,0:T(8,128)(2,1)} %param.35) | copy-start | bytes 6291460
  6.5 5.0 copy-start.10
  6.5 5.1 copy-start.11
  6.5 254.0 %all-gather.17.cloned.1.call-start = ((), (), s32[]{:S(2)}) async-start(), calls=%async_computation.7 | async-start | bytes 1179648 | tf_op jit(solution)/shard_map/all_gather | solution.py:17
  83.9 6.7 %copy-start.7 = (bf16[1024,256]{1,0:T(8,128)(2,1)S(1)}, bf16[1024,256]{1,0:T(8,128)(2,1)}, u32[]{:S(2)}) copy-start(bf16[1024,256]{1,0:T(8,128)(2,1)} %param.24) | copy-start | bytes 1572868
  84.6 180.5 %all-gather.15.cloned.1.call-start = ((), (), s32[]{:S(2)}) async-start(), calls=%async_computation.6 | async-start | bytes 2359296 | tf_op jit(solution)/shard_map/all_gather | solution.py:17
  91.6 8.2 %copy-start.8 = (bf16[1024,256]{1,0:T(8,128)(2,1)S(1)}, bf16[1024,256]{1,0:T(8,128)(2,1)}, u32[]{:S(2)}) copy-start(bf16[1024,256]{1,0:T(8,128)(2,1)} %param.25) | copy-start | bytes 1572868
  212.9 126.6 %reduce-scatter.3.cloned.1.call-start = ((), (), s32[]{:S(2)}) async-start(), calls=%async_computation.2 | async-start | bytes 5242880 | tf_op jit(solution)/shard_map/reduce_scatter | solution.py:172
  212.9 3.0 copy-start.3
  217.2 3.0 copy-start.4
  265.4 5.7 %copy-start.2 = (f32[1024,1,512]{0,2,1:T(8,128)S(1)}, f32[1024,1,512]{0,2,1:T(8,128)}, u32[]{:S(2)}) copy-start(f32[1024,1,512]{0,2,1:T(8,128)} %copy.34) | copy-start | bytes 6291460
  265.4 5.7 %copy-start.9 = (f32[16,64,1,128]{3,1,2,0:T(8,128)S(1)}, f32[16,64,1,128]{3,1,2,0:T(8,128)}, u32[]{:S(2)}) copy-start(f32[16,64,1,128]{3,1,2,0:T(8,128)} %get-tuple-element.194) | copy-start | bytes 1572868
  271.1 2.1 copy-start.6
  271.1 2.1 copy-start.13
  273.2 2.8 copy-start.5
  273.2 2.8 copy-start.12
  281.0 133.2 %all-gather.11.cloned.1.call-start = ((), (), s32[]{:S(2)}) async-start(), calls=%async_computation.3 | async-start | bytes 4718592 | tf_op jit(solution)/shard_map/all_gather | solution.py:145
  281.6 207.7 %all-gather.13.cloned.1.call-start = ((), (), s32[]{:S(2)}) async-start(), calls=%async_computation.4 | async-start | bytes 4718592 | tf_op jit(solution)/shard_map/all_gather | solution.py:146
  282.2 264.3 %reduce-scatter.5.cloned.1.call-start = ((), (), s32[]{:S(2)}) async-start(), calls=%async_computation.5 | async-start | bytes 5242880 | tf_op jit(solution)/shard_map/reduce_scatter | solution.py:186
  347.5 14.3 %collective-permute-start = (bf16[1024,512]{1,0:T(8,128)(2,1)S(1)}, bf16[1024,512]{1,0:T(8,128)(2,1)S(1)}, u32[]{:S(2)}, u32[]{:S(2)}) collective-permute-start(bf16[1024,512]{1,0:T(8,128)(2,1)S(1)} %fusion.75), channel_id=1, source_target_pairs={{0,1},{1,2},{2,3},{3,0},{4,5},{5,6},{6,7},{7,4},{8,9},{9,10},{10,1... | collective-permute-start | bytes 3145736 | tf_op jit(solution)/shard_map/ppermute | solution.py:134
  361.8 14.2 %collective-permute-start.1 = (bf16[1024,512]{1,0:T(8,128)(2,1)S(1)}, bf16[1024,512]{1,0:T(8,128)(2,1)S(1)}, u32[]{:S(2)}, u32[]{:S(2)}) collective-permute-start(bf16[1024,512]{1,0:T(8,128)(2,1)S(1)} %collective-permute-done), channel_id=1, source_target_pairs={{0,1},{1,2},{2,3},{3,0},{4,5},{5,6},{6,7},{7,4},{8,9},{9,10},{10,1... | collective-permute-start | bytes 3145736 | tf_op jit(solution)/shard_map/ppermute | solution.py:134
  376.0 14.3 %collective-permute-start.2 = (bf16[1024,512]{1,0:T(8,128)(2,1)S(1)}, bf16[1024,512]{1,0:T(8,128)(2,1)}, u32[]{:S(2)}, u32[]{:S(2)}) collective-permute-start(bf16[1024,512]{1,0:T(8,128)(2,1)S(1)} %collective-permute-done.1), channel_id=1, source_target_pairs={{0,1},{1,2},{2,3},{3,0},{4,5},{5,6},{6,7},{7,4},{8,9},{9,10},{10,1... | collective-permute-start | bytes 3145736 | tf_op jit(solution)/shard_map/ppermute | solution.py:134
  503.7 45.2 %copy-start.1 = (bf16[512,2048]{1,0:T(8,128)(2,1)S(1)}, bf16[512,2048]{1,0:T(8,128)(2,1)}, u32[]{:S(2)}) copy-start(bf16[512,2048]{1,0:T(8,128)(2,1)} %param.35) | copy-start | bytes 6291460
Sparse Core Ops, SparseCore 0:
  84.7 43.0 all-gather.16
  213.0 52.1 all-gather.14
  281.1 58.2 reduce-scatter.2
  341.4 72.7 all-gather.10
  416.1 73.1 all-gather.12
  503.8 42.5 reduce-scatter.4
